TPU v7x, 32 devices: a whole 2x2x4 slice. The times are simulated.
32 devices in a mesh: rep: 2 (over x), fs: 8 (over z, y), tp: 2 (over core).
Axes of the slice: x: 2, y: 2, z: 4, core: 2. Of those that a mesh axis runs over, the one named last changes fastest.
Arguments:
- stream_in: bfloat16 [16, 1024, 2048], P(('rep', 'fs'), None, 'tp'), may hold values from -48 to 48
- decay_shift: float32 [16, 1024], P(('rep', 'fs')), may hold values from -1.5 to 0, as said below
- mixer_gain: float32 [2048], replicated, may hold values from 0.1 to 1.9
- gate_weight: bfloat16 [2048, 1024], P('fs', 'tp'), may hold values from -0.125 to 0.125
- input_weight: bfloat16 [2048, 1024], P('fs', 'tp'), may hold values from -0.125 to 0.125
- filter_taps: float32 [4, 1024], P(None, 'tp'), may hold values from -3 to 3
- recur_gate: bfloat16 [4, 256, 256], P('tp'), may hold values from -0.375 to 0.375
- inlet_gate: bfloat16 [4, 256, 256], P('tp'), may hold values from -0.375 to 0.375
- decay_param: float32 [1024], P('tp'), may hold values from 1.5 to 12
- mixer_out: bfloat16 [1024, 2048], P('tp', 'fs'), may hold values from -0.1875 to 0.1875
- feedforward_gain: float32 [2048], replicated, may hold values from 0.1 to 1.9
- up_weight: bfloat16 [2048, 4096], P('fs', 'tp'), may hold values from -0.125 to 0.125
- down_weight: bfloat16 [4096, 2048], P('tp', 'fs'), may hold values from -0.09375 to 0.09375
- final_gain: float32 [2048], P('tp'), may hold values from 0.1 to 1.9
Outputs:
- layer_out: bfloat16 [16, 1024, 2048], P(('rep', 'fs'), None, 'tp')
Inputs may be any that keep to these rules, and one draw needn't show every extreme that they name: `decay_shift`: every entry is negative.
All inputs are finite; a program needn't handle non-finite values.
Results may differ from a plain program's by a relative error of at most 0.015.
Values may be sent and summed in bfloat16 or wider, within the bound.
A program may use at most 128 MiB of HBM per device.

v0:
```python
import functools

import jax
import jax.numpy as jnp
from jax import lax
from jax.experimental import pallas as pl
from jax.experimental.pallas import tpu as pltpu
from jax.sharding import PartitionSpec as P

D = 2048


epsilon = 1e-06
rate_scale = 8.0


def norm_rows(values, row_gain):
    mean_sq = jnp.mean(values * values, axis=-1, keepdims=True)
    return values * lax.rsqrt(mean_sq + epsilon) * row_gain


def combine(earlier, later):
    return (earlier[0] * later[0], later[0] * earlier[1] + later[1])


def plain(
    stream_in,
    decay_shift,
    mixer_gain,
    gate_weight,
    input_weight,
    filter_taps,
    recur_gate,
    inlet_gate,
    decay_param,
    mixer_out,
    feedforward_gain,
    up_weight,
    down_weight,
    final_gain,
):
    num_seq, length, half_width = stream_in.shape
    whole = lax.all_gather(stream_in, "tp", axis=2, tiled=True)
    flat_rows = num_seq * length
    normed = norm_rows(whole.reshape(flat_rows, -1).astype(jnp.float32), mixer_gain).astype(
        jnp.bfloat16
    )
    channels = gate_weight.shape[1]
    columns = normed
    gate_logits = jnp.dot(
        columns,
        lax.all_gather(gate_weight, "fs", axis=0, tiled=True),
        preferred_element_type=jnp.float32,
    )
    input_pre = jnp.dot(
        columns,
        lax.all_gather(input_weight, "fs", axis=0, tiled=True),
        preferred_element_type=jnp.float32,
    )
    gate_logits = gate_logits.astype(jnp.bfloat16)
    input_pre = input_pre.astype(jnp.bfloat16)
    branch = jax.nn.gelu(gate_logits.astype(jnp.float32), approximate=True)
    num_taps = filter_taps.shape[0]
    extended_front = jnp.pad(
        input_pre.astype(jnp.float32).reshape(num_seq, length, channels),
        ((0, 0), (num_taps - 1, 0), (0, 0)),
    )
    filtered = jnp.zeros((num_seq, length, channels), jnp.float32)
    for offset in range(num_taps):
        filtered = (
            filtered
            + extended_front[:, offset : offset + length] * filter_taps[offset][None, None, :]
        )
    filtered = filtered.astype(jnp.bfloat16).reshape(flat_rows, channels)
    num_blocks = recur_gate.shape[0]
    grouped = filtered.reshape(flat_rows, num_blocks, recur_gate.shape[1])
    recur = jax.nn.sigmoid(
        jnp.einsum("lni,nij->lnj", grouped, recur_gate, preferred_element_type=jnp.float32).reshape(
            flat_rows, channels
        )
    )
    inlet = jax.nn.sigmoid(
        jnp.einsum("lni,nij->lnj", grouped, inlet_gate, preferred_element_type=jnp.float32).reshape(
            flat_rows, channels
        )
    )
    logarithm_decay = (
        -rate_scale * recur * jax.nn.softplus(-decay_param)[None, :]
        + decay_shift.reshape(flat_rows)[:, None]
    )
    decay = jnp.exp(logarithm_decay).reshape(num_seq, length, channels)
    drive = (
        jnp.sqrt(-jnp.expm1(2.0 * logarithm_decay)) * inlet * filtered.astype(jnp.float32)
    ).reshape(num_seq, length, channels)
    states = lax.associative_scan(combine, (decay, drive), axis=1)[1]
    mixed = (states.reshape(flat_rows, channels) * branch).astype(jnp.bfloat16)
    mixer_terms = (
        jnp.dot(
            mixed,
            lax.all_gather(mixer_out, "fs", axis=1, tiled=True),
            preferred_element_type=jnp.float32,
        )
        .astype(jnp.bfloat16)
        .astype(jnp.float32)
    )
    mixer_sum = lax.psum_scatter(
        mixer_terms.astype(jnp.bfloat16), "tp", scatter_dimension=1, tiled=True
    ).astype(jnp.float32)
    stream_mid = (stream_in.reshape(flat_rows, half_width).astype(jnp.float32) + mixer_sum).astype(
        jnp.bfloat16
    )
    stream_whole = lax.all_gather(stream_mid, "tp", axis=1, tiled=True)
    normed_mid = norm_rows(stream_whole.astype(jnp.float32), feedforward_gain).astype(jnp.bfloat16)
    columns = normed_mid
    up_proj = jnp.dot(
        columns,
        lax.all_gather(up_weight, "fs", axis=0, tiled=True),
        preferred_element_type=jnp.float32,
    )
    activated = jnp.square(jax.nn.relu(up_proj)).astype(jnp.bfloat16)
    ffn_terms = (
        jnp.dot(
            activated,
            lax.all_gather(down_weight, "fs", axis=1, tiled=True),
            preferred_element_type=jnp.float32,
        )
        .astype(jnp.bfloat16)
        .astype(jnp.float32)
    )
    ffn_sum = lax.psum_scatter(
        ffn_terms.astype(jnp.bfloat16), "tp", scatter_dimension=1, tiled=True
    ).astype(jnp.float32)
    total = stream_mid.astype(jnp.float32) + ffn_sum
    squares_sum = lax.psum(jnp.sum(total * total, axis=1), "tp")
    layer_out = total * lax.rsqrt(squares_sum / D + epsilon)[:, None] * final_gain[None, :]
    return layer_out.astype(jnp.bfloat16).reshape(num_seq, length, half_width)


F32 = jnp.float32
BF16 = jnp.bfloat16
TILE = 16
ROWS = 256


def split_rows(rows, up):
    third = rows // 3 // TILE * TILE + (TILE if up else 0)
    return rows - 2 * third, third


def expm1_neg(v):
    series = -v * (1.0 + v * (1 / 2) * (1.0 + v * (1 / 3) * (1.0 + v * (1 / 4) * (1.0 + v * (1 / 5) * (1.0 + v * (1 / 6))))))
    return jnp.where(v > -0.25, series, 1.0 - jnp.exp(v))


def layer_kernel(
    n,
    x_in, shift_ref, mgain_ref, wg_in, wi_in, taps_ref, rg_ref, ig_ref, sp_ref, wo_in,
    fgain_ref, wu_in, wd_in,
    out_ref, scale_ref,
    x_ref, wg, wi, wo, wu, wd, other, normed, front, carry, scan_a, scan_b, part, prec, mid, mid_other,
    act, sq_send, sq_recv,
    local_sems, send_sems, recv_sems, tp_send, tp_recv,
):
    rep, fs, tp = lax.axis_index("rep"), lax.axis_index("fs"), lax.axis_index("tp")
    half_n = n // 2
    length, half = x_in.shape
    channels = wg.shape[1]
    width = wd.shape[2]
    shard = wg_in.shape[0]
    hidden = wu.shape[1]
    blocks = length // ROWS

    def ring_to_fs(p):
        p = lax.rem(p + 2 * n, n)
        return jnp.where(p < half_n, 2 * p, 2 * (n - 1 - p) + 1)

    odd = lax.rem(fs, 2)
    pos = (1 - odd) * (fs // 2) + odd * (n - 1 - fs // 2)
    right, left = ring_to_fs(pos + 1), ring_to_fs(pos - 1)

    def by_row(dst, lo, cols):
        def view(owner, off, size):
            return dst.at[pl.ds(pl.multiple_of(owner * shard + off, TILE), size), pl.ds(lo, cols)]
        return view

    def by_owner(dst, lo):
        def view(owner, off, size):
            return dst.at[owner, pl.ds(pl.multiple_of(lo + off, TILE), size), :]
        return view

    rows_o, rows_d = wo.shape[1], wd.shape[1]
    views = [
        (by_row(wg, 0, channels), split_rows(shard, False)),
        (by_row(wi, 0, channels), split_rows(shard, False)),
        (by_owner(wo, 0), split_rows(rows_o, True)),
        (by_row(wu, 0, hidden // 2), split_rows(shard, True)),
        (by_row(wu, hidden // 2, hidden // 2), split_rows(shard, False)),
        (by_owner(wd, 0), split_rows(rows_d // 2, False)),
        (by_owner(wd, rows_d // 2), split_rows(rows_d // 2, False)),
    ]

    def remote(view, k, lane, s, device):
        return pltpu.make_async_remote_copy(
            src_ref=view, dst_ref=view, send_sem=send_sems.at[k, lane, s],
            recv_sem=recv_sems.at[k, lane, s], device_id=device,
            device_id_type=pl.DeviceIdType.MESH,
        )

    def cw(k, s, shift=0):
        view, (p, _) = views[k]
        return remote(view(ring_to_fs(pos - s - shift), 0, p), k, 0, s, {"fs": right})

    def ccw(k, s, shift=0):
        view, (p, q) = views[k]
        return remote(view(ring_to_fs(pos + s + shift), p + rep * q, q), k, 1, s, {"fs": left})

    def across(k, s, side):
        view, (p, q) = views[k]
        return remote(view(ring_to_fs(pos + s + 1), p + side * q, q), k, 2, s, {"rep": 1 - rep})

    def begin(k):
        cw(k, 0).start()
        ccw(k, 0).start()

    def service(k, s, last):
        cw(k, s, 1).wait_recv()

        def forward(make):
            if last is None:
                pl.when(s + 1 < n - 1)(lambda: make(k, s + 1).start())
            elif not last:
                make(k, s + 1).start()

        forward(cw)
        ccw(k, s, 1).wait_recv()
        forward(ccw)
        across(k, s, rep).start()

    def wait_across(k, s):
        across(k, s, 1 - rep).wait_recv()

    def swap(src, dst, index):
        return pltpu.make_async_remote_copy(
            src_ref=src, dst_ref=dst, send_sem=tp_send.at[index], recv_sem=tp_recv.at[index],
            device_id={"tp": 1 - tp}, device_id_type=pl.DeviceIdType.MESH,
        )

    own = [
        (x_in, x_ref),
        (wg_in, wg.at[pl.ds(pl.multiple_of(fs * shard, TILE), shard), :]),
        (wi_in, wi.at[pl.ds(pl.multiple_of(fs * shard, TILE), shard), :]),
        (wo_in, wo.at[fs]),
        (wu_in, wu.at[pl.ds(pl.multiple_of(fs * shard, TILE), shard), :]),
        (wd_in, wd.at[fs]),
    ]
    local = [pltpu.make_async_copy(a, b, local_sems.at[i]) for i, (a, b) in enumerate(own)]
    for i in (1, 2, 3, 0, 4, 5):
        local[i].start()
    barrier = pltpu.get_barrier_semaphore()
    for device in ({"fs": right}, {"fs": left}, {"rep": 1 - rep}, {"tp": 1 - tp}):
        pl.semaphore_signal(barrier, inc=1, device_id=device, device_id_type=pl.DeviceIdType.MESH)
    pl.semaphore_wait(barrier, 4)
    swap_x = swap(x_ref, other, 0)
    for k in range(3):
        local[1 + k].wait()
        begin(k)
    local[0].wait()
    swap_x.start()
    local[4].wait()
    local[5].wait()

    own_cols = pl.ds(pl.multiple_of(tp * half, 128), half)
    other_cols = pl.ds(pl.multiple_of((1 - tp) * half, 128), half)

    def norm_block(first, second, gain_ref, rows):
        a = first[rows, :].astype(F32)
        b = second[rows, :].astype(F32)
        mean = (jnp.sum(a * a, axis=1, keepdims=True) + jnp.sum(b * b, axis=1, keepdims=True)) / (2 * half)
        scale = lax.rsqrt(mean + epsilon)
        normed[rows, own_cols] = (a * scale * gain_ref[:, own_cols]).astype(BF16)
        normed[rows, other_cols] = (b * scale * gain_ref[:, other_cols]).astype(BF16)

    small = 64

    pieces = length // small
    share = -(-pieces // (n - 2))

    @pl.loop(0, n - 2)
    def _(s):
        for k in range(3):
            service(k, s, False)
        pl.when(s == 0)(swap_x.wait)
        pl.when(s == n - 3)(lambda: begin(3))
        for piece in range(share):
            i = s * share + piece

            @pl.when(i < pieces)
            def _():
                norm_block(x_ref, other, mgain_ref, pl.ds(pl.multiple_of(i * small, small), small))

    begin(4)
    for k in range(3):
        service(k, n - 2, True)

    @pl.loop(0, n - 1)
    def _(s):
        for k in range(3):
            wait_across(k, s)

    front[pl.ds(0, 8), :] = jnp.zeros((8, channels), F32)
    carry[...] = jnp.zeros_like(carry)
    decay_param = sp_ref[...]
    rate = rate_scale * (jnp.maximum(-decay_param, 0.0) + jnp.log1p(jnp.exp(-jnp.abs(decay_param))))
    num_taps = taps_ref.shape[0]
    groups = rg_ref.shape[0]
    block = rg_ref.shape[1]
    per = n // blocks
    lead = n - 2

    def tick(t):
        @pl.when(t < n - 1)
        def _():
            for k in (3, 4):
                service(k, t, None)

        pl.when(t == n - 4)(lambda: begin(5))
        pl.when(t == n - 3)(lambda: begin(6))

        @pl.when(t >= lead)
        def _():
            for k in (5, 6):
                service(k, t - lead, None)

    @pl.loop(0, blocks)
    def _(i):
        rows = pl.ds(pl.multiple_of(i * ROWS, ROWS), ROWS)
        for step in range(per - per // 2):
            tick(i * per + step)
        cols = normed[rows, :]
        front[pl.ds(8, ROWS), :] = jnp.dot(cols, wi[...], preferred_element_type=F32).astype(BF16).astype(F32)
        gate = jnp.dot(cols, wg[...], preferred_element_type=F32).astype(BF16)
        shift = jnp.transpose(jnp.broadcast_to(shift_ref[:, rows], (128, ROWS)))[:, :1]
        for g in range(groups):
            ch = slice(g * block, (g + 1) * block)
            window = front[:, ch]
            filtered = jnp.zeros((ROWS, block), F32)
            for tap in range(num_taps):
                back = num_taps - 1 - tap
                moved = window if back == 0 else pltpu.roll(window, back, 0)
                filtered = filtered + moved[8:] * taps_ref[tap : tap + 1, ch]
            filtered = filtered.astype(BF16)
            recur = jax.nn.sigmoid(jnp.dot(filtered, rg_ref[g], preferred_element_type=F32))
            inlet = jax.nn.sigmoid(jnp.dot(filtered, ig_ref[g], preferred_element_type=F32))
            log_decay = shift - recur * rate[:, ch]
            a = jnp.exp(log_decay)
            b = jnp.sqrt(expm1_neg(2.0 * log_decay)) * inlet * filtered.astype(F32)
            a = a.reshape(ROWS // 8, 8, block)
            b = b.reshape(ROWS // 8, 8, block)
            at = lax.broadcasted_iota(jnp.int32, (ROWS // 8, 8, block), 1)
            for back in (1, 2, 4):
                keep = at >= back
                b = jnp.where(keep, a * pltpu.roll(b, back, 1) + b, b)
                a = jnp.where(keep, a * pltpu.roll(a, back, 1), a)
            scan_a[:, ch] = a.reshape(ROWS, block)
            scan_b[:, ch] = b.reshape(ROWS, block)
        front[pl.ds(0, 8), :] = front[pl.ds(ROWS, 8), :]

        def step_scan(t, h):
            at = pl.ds(pl.multiple_of(t * 8, 8), 8)
            states = scan_a[at, :] * h + scan_b[at, :]
            scan_b[at, :] = states
            return jnp.broadcast_to(states[7:8, :], states.shape)

        carry[...] = lax.fori_loop(0, ROWS // 8, step_scan, carry[...], unroll=4)
        for step in range(per - per // 2, per):
            tick(i * per + step)
        mixed = (scan_b[...] * jax.nn.gelu(gate.astype(F32), approximate=True)).astype(BF16)
        for j in range(half_n):
            to = pl.ds(j * width, width)
            part[1, rows, to] = jnp.dot(mixed, wo[(1 - tp) * half_n + j], preferred_element_type=F32).astype(BF16)
        swap(part.at[1, rows, :], prec.at[rows, :], 1 + i).start()
        for j in range(half_n):
            to = pl.ds(j * width, width)
            part[0, rows, to] = jnp.dot(mixed, wo[tp * half_n + j], preferred_element_type=F32).astype(BF16)

    @pl.loop(0, blocks)
    def _(i):
        rows = pl.ds(pl.multiple_of(i * ROWS, ROWS), ROWS)
        swap(part.at[1, rows, :], prec.at[rows, :], 1 + i).wait()
        mid[rows, :] = (
            x_ref[rows, :].astype(F32) + (part[0, rows, :].astype(F32) + prec[rows, :].astype(F32))
        ).astype(BF16)
        swap(mid.at[rows, :], mid_other.at[rows, :], 1 + blocks + i).start()

    at_tick = per * blocks
    tick(at_tick)

    @pl.loop(0, blocks)
    def _(i):
        rows = pl.ds(pl.multiple_of(i * ROWS, ROWS), ROWS)
        swap(mid.at[rows, :], mid_other.at[rows, :], 1 + blocks + i).wait()

    @pl.loop(0, length // small)
    def _(i):
        norm_block(mid, mid_other, fgain_ref, pl.ds(pl.multiple_of(i * small, small), small))

    @pl.loop(0, n - 1)
    def _(s):
        for k in (3, 4):
            wait_across(k, s)

    tick(at_tick + 1)

    up_cols = min(512, hidden)
    late = (2 * n - 4 - at_tick - 2) // (hidden // up_cols // 2)
    done = at_tick + 2 + late * (hidden // up_cols // 2) - lead

    @pl.loop(0, hidden // up_cols)
    def _(c):
        to = pl.ds(pl.multiple_of(c * up_cols, up_cols), up_cols)

        @pl.loop(0, blocks)
        def _(i):
            rows = pl.ds(pl.multiple_of(i * ROWS, ROWS), ROWS)
            up = jnp.maximum(jnp.dot(normed[rows, :], wu[:, to], preferred_element_type=F32), 0.0)
            act[rows, to] = (up * up).astype(BF16)

        @pl.when(lax.rem(c, 2) == 1)
        def _():
            for step in range(late):
                tick(at_tick + 2 + (c // 2) * late + step)

    def back_swap(column):
        to = pl.ds(pl.multiple_of(column * width, 128), width)
        return swap(part.at[1, :, to], prec.at[:, to], 1 + 2 * blocks + column)

    def down_block(owner):
        column = lax.rem(owner, half_n)
        slot = lax.rem(owner // half_n + tp, 2)
        to = pl.ds(pl.multiple_of(column * width, 128), width)

        @pl.loop(0, blocks)
        def _(i):
            rows = pl.ds(pl.multiple_of(i * ROWS, ROWS), ROWS)
            part[slot, rows, to] = jnp.dot(act[rows, :], wd[owner], preferred_element_type=F32).astype(BF16)

        @pl.when(slot == 1)
        def _():
            back_swap(column).start()

    down_block(fs)
    for s in range(half_n - 1, n - 1):
        if s >= done:
            tick(s + lead)
        for earlier in range(half_n) if s == half_n - 1 else [s]:
            for k in (5, 6):
                wait_across(k, earlier)
        for ahead in [s + 1] if s == half_n - 1 else [-s - 1, s + 1]:
            down_block(ring_to_fs(pos + ahead))
    for j in range(half_n):
        back_swap(j).wait()

    @pl.loop(0, length // small)
    def _(i):
        rows = pl.ds(pl.multiple_of(i * small, small), small)
        total = mid[rows, :].astype(F32) + (part[0, rows, :].astype(F32) + prec[rows, :].astype(F32))
        out_ref[rows, :] = total.astype(BF16)
        sq_send[rows, :] = jnp.broadcast_to(jnp.sum(total * total, axis=1, keepdims=True), (small, 128))

    swap_sq = swap(sq_send, sq_recv, 1 + 2 * blocks + half_n)
    swap_sq.start()
    swap_sq.wait()
    scale_ref[...] = lax.rsqrt((sq_send[...] + sq_recv[...]) / (2 * half) + epsilon)

    @pl.loop(0, n - 1)
    def _(s):
        for k in range(len(views)):
            cw(k, s).wait_send()
            ccw(k, s).wait_send()
            across(k, s, rep).wait_send()


def closing_kernel(total_ref, scale_ref, gain_ref, out_ref):
    out_ref[...] = (total_ref[...].astype(F32) * scale_ref[:, :1] * gain_ref[...]).astype(BF16)


def fused(n, stream_in, decay_shift, mixer_gain, gate_weight, input_weight, filter_taps, recur_gate,
          inlet_gate, decay_param, mixer_out, feedforward_gain, up_weight, down_weight, final_gain):
    _, length, half = stream_in.shape
    shard, channels = gate_weight.shape
    hidden = up_weight.shape[1]
    width = down_weight.shape[1]
    model = shard * n
    blocks = length // ROWS
    half_n = n // 2
    vmem = pl.BlockSpec(memory_space=pltpu.VMEM)
    hbm = pl.BlockSpec(memory_space=pl.ANY)
    swaps = 2 + 2 * blocks + half_n
    total, scale = pl.pallas_call(
        functools.partial(layer_kernel, n),
        out_shape=(jax.ShapeDtypeStruct((length, half), BF16), jax.ShapeDtypeStruct((length, 128), F32)),
        in_specs=[hbm, vmem, vmem, hbm, hbm, vmem, vmem, vmem, vmem, hbm, vmem, hbm, hbm],
        out_specs=(vmem, vmem),
        scratch_shapes=[
            pltpu.VMEM((length, half), BF16),
            pltpu.VMEM((model, channels), BF16),
            pltpu.VMEM((model, channels), BF16),
            pltpu.VMEM((n, channels, width), BF16),
            pltpu.VMEM((model, hidden), BF16),
            pltpu.VMEM((n, hidden, width), BF16),
            pltpu.VMEM((length, half), BF16),
            pltpu.VMEM((length, model), BF16),
            pltpu.VMEM((8 + ROWS, channels), F32),
            pltpu.VMEM((8, channels), F32),
            pltpu.VMEM((ROWS, channels), F32),
            pltpu.VMEM((ROWS, channels), F32),
            pltpu.VMEM((2, length, half), BF16),
            pltpu.VMEM((length, half), BF16),
            pltpu.VMEM((length, half), BF16),
            pltpu.VMEM((length, half), BF16),
            pltpu.VMEM((length, hidden), BF16),
            pltpu.VMEM((length, 128), F32),
            pltpu.VMEM((length, 128), F32),
            pltpu.SemaphoreType.DMA((6,)),
            pltpu.SemaphoreType.DMA((7, 3, n - 1)),
            pltpu.SemaphoreType.DMA((7, 3, n - 1)),
            pltpu.SemaphoreType.DMA((swaps,)),
            pltpu.SemaphoreType.DMA((swaps,)),
        ],
        compiler_params=pltpu.CompilerParams(
            collective_id=0, has_side_effects=True, vmem_limit_bytes=67043328
        ),
        name="gated_layer",
    )(
        stream_in.reshape(length, half),
        decay_shift,
        mixer_gain.reshape(1, -1),
        gate_weight,
        input_weight,
        filter_taps,
        recur_gate,
        inlet_gate,
        decay_param.reshape(1, -1),
        mixer_out,
        feedforward_gain.reshape(1, -1),
        up_weight,
        down_weight,
    )
    tile = pl.BlockSpec((ROWS, half), lambda i: (i, 0))
    out = pl.pallas_call(
        closing_kernel,
        grid=(blocks,),
        out_shape=jax.ShapeDtypeStruct((length, half), BF16),
        in_specs=[
            tile,
            pl.BlockSpec((ROWS, 128), lambda i: (i, 0)),
            pl.BlockSpec((1, half), lambda i: (0, 0)),
        ],
        out_specs=tile,
        name="closing",
    )(total, scale, final_gain.reshape(1, -1))
    return out.reshape(1, length, half)


def fits(mesh, n, args):
    num_seq, length, half = args[0].shape
    width = args[9].shape[1]
    shard = args[3].shape[0]
    return (
        mesh.shape["rep"] == 2 and mesh.shape["tp"] == 2 and n % 8 == 0 and num_seq == 1
        and width % 128 == 0 and args[11].shape[1] % 1024 == 0 and length == 4 * ROWS and shard >= 3 * TILE and length % ROWS == 0
    )


def local_for(mesh):
    n = mesh.shape["fs"]

    def local(*args):
        if fits(mesh, n, args):
            return fused(n, *args)
        return plain(*args)

    return local


def solution(mesh):
    return jax.shard_map(
        local_for(mesh),
        mesh=mesh,
        in_specs=(
            P(("rep", "fs"), None, "tp"),
            P(("rep", "fs"), None),
            P(),
            P("fs", "tp"),
            P("fs", "tp"),
            P(None, "tp"),
            P("tp", None, None),
            P("tp", None, None),
            P("tp"),
            P("tp", "fs"),
            P(),
            P("fs", "tp"),
            P("tp", "fs"),
            P("tp"),
        ),
        out_specs=P(("rep", "fs"), None, "tp"),
        check_vma=False,
    )
```

profile of v0, /device:TPU:0, one launch (start us, length us, event | category | flops | bytes accessed | tf_op | source)
XLA Modules:
  0.0 180.8 jit_solution(9090353928096744736)
XLA Ops:
  0.0 176.6 %gated_layer.1 = (bf16[1024,1024]{1,0:T(8,128)(2,1)}, f32[1024,128]{1,0:T(8,128)}) custom-call(bf16[1024,1024]{1,0:T(8,128)(2,1)} %bitcast.6, f32[1,1024]{1,0:T(1,128)} %shift_ref.1, f32[1,2048]{1,0:T(1,128)} %bitcast.7, bf16[256,512]{1,0:T(8,128)(2,1)} %wg_in.1, bf16[256,512]{1,0:T(8,128)(2,1)} %wi_in.1, f32[4,512]{1,0:T(4,128)} %taps_ref.1, ...), custom_call_target="tpu_custom_call" | custom-call | tf_op jit(solution)/shard_map/gated_layer/pallas_call | solution.py:499
  176.6 4.1 %closing.1 = bf16[1024,1024]{1,0:T(8,128)(2,1)} custom-call(bf16[1024,1024]{1,0:T(8,128)(2,1)} %get-tuple-element.7.total_ref, f32[1024,128]{1,0:T(8,128)} %get-tuple-element.8.scale_ref, f32[1,1024]{1,0:T(1,128)} %bitcast.9), custom_call_target="tpu_custom_call" | custom-call | tf_op jit(solution)/shard_map/closing/pallas_call | solution.py:550
where the time goes:
time: 181 us
  Pallas kernels  181 us (100%)
    pallas_call x1, Pallas kernels, fused(): pl.pallas_call(functools.partial(layer_kernel, n), out_shape=(jax.ShapeDt...  177 us
    pallas_call x1, Pallas kernels, fused(): pl.pallas_call(closing_kernel, grid=(blocks,), out_shape=jax.ShapeDtypeSt...  4.15 us

commit v1 on v0

--- a/solution.py
+++ b/solution.py
@@ -139,6 +139,7 @@
 F32 = jnp.float32
 BF16 = jnp.bfloat16
 TILE = 16
+FORE, BACK, BOTH = range(3)
 ROWS = 256
 
 
@@ -159,7 +160,7 @@
     out_ref, scale_ref,
     x_ref, wg, wi, wo, wu, wd, other, normed, front, carry, scan_a, scan_b, part, prec, mid, mid_other,
     act, sq_send, sq_recv,
-    local_sems, send_sems, recv_sems, tp_send, tp_recv,
+    local_sems, send_sems, recv_sems, tp_send, tp_recv, out_sems,
 ):
     rep, fs, tp = lax.axis_index("rep"), lax.axis_index("fs"), lax.axis_index("tp")
     half_n = n // 2
@@ -189,15 +190,23 @@
         return view
 
     rows_o, rows_d = wo.shape[1], wd.shape[1]
+    cut = hidden * 3 // 8
+    rest = (hidden - cut) // 2
+    last = rows_d // 16
+    main = (rows_d - 2 * last) // 2
     views = [
-        (by_row(wg, 0, channels), split_rows(shard, False)),
-        (by_row(wi, 0, channels), split_rows(shard, False)),
-        (by_owner(wo, 0), split_rows(rows_o, True)),
-        (by_row(wu, 0, hidden // 2), split_rows(shard, True)),
-        (by_row(wu, hidden // 2, hidden // 2), split_rows(shard, False)),
-        (by_owner(wd, 0), split_rows(rows_d // 2, False)),
-        (by_owner(wd, rows_d // 2), split_rows(rows_d // 2, False)),
+        (by_row(wg, 0, channels), BACK, split_rows(shard, True)),
+        (by_row(wi, 0, channels), FORE, split_rows(shard, True)),
+        (by_owner(wo, 0), FORE, split_rows(rows_o, False)),
+        (by_row(wu, 0, cut), BACK, split_rows(shard, True)),
+        (by_row(wu, cut, rest), FORE, split_rows(shard, True)),
+        (by_row(wu, cut + rest, rest), BACK, split_rows(shard, False)),
+        (by_owner(wd, 0), FORE, split_rows(main, False)),
+        (by_owner(wd, main), BACK, split_rows(main, False)),
+        (by_owner(wd, 2 * main), BOTH, (last, last)),
     ]
+    ups = range(3, 6)
+    downs = range(6, 9)
 
     def remote(view, k, lane, s, device):
         return pltpu.make_async_remote_copy(
@@ -207,37 +216,46 @@
         )
 
     def cw(k, s, shift=0):
-        view, (p, _) = views[k]
-        return remote(view(ring_to_fs(pos - s - shift), 0, p), k, 0, s, {"fs": right})
+        view, role, (p, q) = views[k]
+        lo, size = (p + rep * q, q) if role == BACK else (0, p)
+        return remote(view(ring_to_fs(pos - s - shift), lo, size), k, 0, s, {"fs": right})
 
     def ccw(k, s, shift=0):
-        view, (p, q) = views[k]
-        return remote(view(ring_to_fs(pos + s + shift), p + rep * q, q), k, 1, s, {"fs": left})
+        view, role, (p, q) = views[k]
+        lo, size = (p + rep * q, q) if role == FORE else (p if role == BOTH else 0, q if role == BOTH else p)
+        return remote(view(ring_to_fs(pos + s + shift), lo, size), k, 1, s, {"fs": left})
 
     def across(k, s, side):
-        view, (p, q) = views[k]
-        return remote(view(ring_to_fs(pos + s + 1), p + side * q, q), k, 2, s, {"rep": 1 - rep})
+        view, role, (p, q) = views[k]
+        owner = pos + s + 1 if role == FORE else pos - s - 1
+        return remote(view(ring_to_fs(owner), p + side * q, q), k, 2, s, {"rep": 1 - rep})
+
+    def shared(k):
+        return views[k][1] != BOTH
 
     def begin(k):
         cw(k, 0).start()
         ccw(k, 0).start()
 
     def service(k, s, last):
-        cw(k, s, 1).wait_recv()
-
         def forward(make):
             if last is None:
                 pl.when(s + 1 < n - 1)(lambda: make(k, s + 1).start())
             elif not last:
                 make(k, s + 1).start()
 
+        cw(k, s, 1).wait_recv()
         forward(cw)
+        if views[k][1] == BACK:
+            across(k, s, rep).start()
         ccw(k, s, 1).wait_recv()
         forward(ccw)
-        across(k, s, rep).start()
+        if views[k][1] == FORE:
+            across(k, s, rep).start()
 
     def wait_across(k, s):
-        across(k, s, 1 - rep).wait_recv()
+        if shared(k):
+            across(k, s, 1 - rep).wait_recv()
 
     def swap(src, dst, index):
         return pltpu.make_async_remote_copy(
@@ -290,7 +308,8 @@
         for k in range(3):
             service(k, s, False)
         pl.when(s == 0)(swap_x.wait)
-        pl.when(s == n - 3)(lambda: begin(3))
+        for k in list(ups)[:2]:
+            pl.when(s == n - 3)(functools.partial(begin, k))
         for piece in range(share):
             i = s * share + piece
 
@@ -298,9 +317,21 @@
             def _():
                 norm_block(x_ref, other, mgain_ref, pl.ds(pl.multiple_of(i * small, small), small))
 
-    begin(4)
+    begin(ups[-1])
     for k in range(3):
         service(k, n - 2, True)
+
+    lead = n - 2
+
+    def tick(t, j):
+        pl.when(t < n - 1)(lambda: service(ups[j], t, None))
+        if j == 2:
+            for e, k in enumerate(downs):
+                pl.when(t == (n - 4 if e == 0 else n - 3))(functools.partial(begin, k))
+        pl.when(t >= lead)(lambda: service(downs[j], t - lead, None))
+
+    for j in range(3):
+        tick(0, j)
 
     @pl.loop(0, n - 1)
     def _(s):
@@ -314,33 +345,17 @@
     num_taps = taps_ref.shape[0]
     groups = rg_ref.shape[0]
     block = rg_ref.shape[1]
-    per = n // blocks
-    lead = n - 2
-
-    def tick(t):
-        @pl.when(t < n - 1)
-        def _():
-            for k in (3, 4):
-                service(k, t, None)
-
-        pl.when(t == n - 4)(lambda: begin(5))
-        pl.when(t == n - 3)(lambda: begin(6))
-
-        @pl.when(t >= lead)
-        def _():
-            for k in (5, 6):
-                service(k, t - lead, None)
-
     @pl.loop(0, blocks)
     def _(i):
         rows = pl.ds(pl.multiple_of(i * ROWS, ROWS), ROWS)
-        for step in range(per - per // 2):
-            tick(i * per + step)
+        tick(i + 1, 0)
         cols = normed[rows, :]
         front[pl.ds(8, ROWS), :] = jnp.dot(cols, wi[...], preferred_element_type=F32).astype(BF16).astype(F32)
         gate = jnp.dot(cols, wg[...], preferred_element_type=F32).astype(BF16)
         shift = jnp.transpose(jnp.broadcast_to(shift_ref[:, rows], (128, ROWS)))[:, :1]
         for g in range(groups):
+            if g == 1:
+                tick(i + 1, 1)
             ch = slice(g * block, (g + 1) * block)
             window = front[:, ch]
             filtered = jnp.zeros((ROWS, block), F32)
@@ -372,8 +387,7 @@
             return jnp.broadcast_to(states[7:8, :], states.shape)
 
         carry[...] = lax.fori_loop(0, ROWS // 8, step_scan, carry[...], unroll=4)
-        for step in range(per - per // 2, per):
-            tick(i * per + step)
+        tick(i + 1, 2)
         mixed = (scan_b[...] * jax.nn.gelu(gate.astype(F32), approximate=True)).astype(BF16)
         for j in range(half_n):
             to = pl.ds(j * width, width)
@@ -383,6 +397,8 @@
             to = pl.ds(j * width, width)
             part[0, rows, to] = jnp.dot(mixed, wo[tp * half_n + j], preferred_element_type=F32).astype(BF16)
 
+    tick(blocks + 1, 0)
+
     @pl.loop(0, blocks)
     def _(i):
         rows = pl.ds(pl.multiple_of(i * ROWS, ROWS), ROWS)
@@ -392,29 +408,34 @@
         ).astype(BF16)
         swap(mid.at[rows, :], mid_other.at[rows, :], 1 + blocks + i).start()
 
-    at_tick = per * blocks
-    tick(at_tick)
+    tick(blocks + 1, 1)
 
     @pl.loop(0, blocks)
     def _(i):
         rows = pl.ds(pl.multiple_of(i * ROWS, ROWS), ROWS)
         swap(mid.at[rows, :], mid_other.at[rows, :], 1 + blocks + i).wait()
 
-    @pl.loop(0, length // small)
-    def _(i):
-        norm_block(mid, mid_other, fgain_ref, pl.ds(pl.multiple_of(i * small, small), small))
+    tick(blocks + 1, 2)
+
+    for part_of in range(2):
+
+        @pl.loop(part_of * (pieces // 2), (part_of + 1) * (pieces // 2))
+        def _(i):
+            norm_block(mid, mid_other, fgain_ref, pl.ds(pl.multiple_of(i * small, small), small))
+
+        tick(blocks + 2, part_of)
+
+    tick(blocks + 2, 2)
+    for t in range(blocks + 3, n):
+        for j in range(3):
+            tick(t, j)
 
     @pl.loop(0, n - 1)
     def _(s):
-        for k in (3, 4):
+        for k in ups:
             wait_across(k, s)
 
-    tick(at_tick + 1)
-
     up_cols = min(512, hidden)
-    late = (2 * n - 4 - at_tick - 2) // (hidden // up_cols // 2)
-    done = at_tick + 2 + late * (hidden // up_cols // 2) - lead
-
     @pl.loop(0, hidden // up_cols)
     def _(c):
         to = pl.ds(pl.multiple_of(c * up_cols, up_cols), up_cols)
@@ -425,63 +446,133 @@
             up = jnp.maximum(jnp.dot(normed[rows, :], wu[:, to], preferred_element_type=F32), 0.0)
             act[rows, to] = (up * up).astype(BF16)
 
-        @pl.when(lax.rem(c, 2) == 1)
-        def _():
-            for step in range(late):
-                tick(at_tick + 2 + (c // 2) * late + step)
-
-    def back_swap(column):
-        to = pl.ds(pl.multiple_of(column * width, 128), width)
-        return swap(part.at[1, :, to], prec.at[:, to], 1 + 2 * blocks + column)
-
-    def down_block(owner):
+        for j in range(3):
+            pl.when(c == j)(functools.partial(tick, n, j))
+
+    tick(n + 1, 0)
+
+    def place(owner, i):
         column = lax.rem(owner, half_n)
         slot = lax.rem(owner // half_n + tp, 2)
+        rows = pl.ds(pl.multiple_of(i * ROWS, ROWS), ROWS)
         to = pl.ds(pl.multiple_of(column * width, 128), width)
-
+        return column, slot, rows, to
+
+    def back_swap(column, i):
+        _, _, rows, to = place(column, i)
+        return swap(part.at[1, rows, to], prec.at[rows, to], 1 + 2 * blocks + column * blocks + i)
+
+    def write(column, i):
+        _, _, rows, to = place(column, i)
+        return pltpu.make_async_copy(other.at[rows, to], out_ref.at[rows, to], out_sems.at[column * blocks + i])
+
+    def down_rows(owner, i):
+        column, slot, rows, to = place(owner, i)
+        part[slot, rows, to] = jnp.dot(act[rows, :], wd[owner], preferred_element_type=F32).astype(BF16)
+        pl.when(slot == 1)(lambda: back_swap(column, i).start())
+
+    def total_rows(owner, i):
+        column, slot, rows, to = place(owner, i)
+
+        @pl.when(slot == 0)
+        def _():
+            back_swap(column, i).wait_recv()
+            total = mid[rows, to].astype(F32) + (part[0, rows, to].astype(F32) + prec[rows, to].astype(F32))
+            other[rows, to] = total.astype(BF16)
+            squares = total * total
+            sq_send[rows, :] += sum(squares[:, at : at + 128] for at in range(0, width, 128))
+            write(column, i).start()
+
+    def over_rows(*makes):
         @pl.loop(0, blocks)
         def _(i):
-            rows = pl.ds(pl.multiple_of(i * ROWS, ROWS), ROWS)
-            part[slot, rows, to] = jnp.dot(act[rows, :], wd[owner], preferred_element_type=F32).astype(BF16)
-
-        @pl.when(slot == 1)
-        def _():
-            back_swap(column).start()
-
-    down_block(fs)
+            for make, owner in makes:
+                make(owner, i)
+
+    order = [ring_to_fs(pos + ahead) for ahead in [0, half_n]]
+    for s in range(half_n, n - 1):
+        order += [ring_to_fs(pos - s - 1), ring_to_fs(pos + s + 1)]
+    sq_send[...] = jnp.zeros_like(sq_send)
+    over_rows((down_rows, order[0]))
+    for at in range(3 * n + 4, 3 * (lead + half_n + 1)):
+        tick(at // 3, at % 3)
     for s in range(half_n - 1, n - 1):
-        if s >= done:
-            tick(s + lead)
+        ahead = lead + s + 2
         for earlier in range(half_n) if s == half_n - 1 else [s]:
-            for k in (5, 6):
+            for k in downs:
                 wait_across(k, earlier)
-        for ahead in [s + 1] if s == half_n - 1 else [-s - 1, s + 1]:
-            down_block(ring_to_fs(pos + ahead))
-    for j in range(half_n):
-        back_swap(j).wait()
-
-    @pl.loop(0, length // small)
+        if s == half_n - 1:
+            over_rows((down_rows, order[1]), (total_rows, order[0]))
+        elif s < n - 2:
+            at = 2 * (s - half_n + 1)
+            over_rows((down_rows, order[at]), (total_rows, order[at - 1]))
+            if s < n - 3:
+                tick(ahead, 0)
+            over_rows((down_rows, order[at + 1]), (total_rows, order[at]))
+        if s < n - 3:
+            for j in range(1 if s >= half_n else 0, 3):
+                tick(ahead, j)
+    over_rows((down_rows, order[-2]), (down_rows, order[-1]), (total_rows, order[-3]))
+
+    def swap_sq(i):
+        rows = pl.ds(pl.multiple_of(i * ROWS, ROWS), ROWS)
+        return swap(sq_send.at[rows, :], sq_recv.at[rows, :], 1 + 2 * blocks + half_n * blocks + i)
+
+    @pl.loop(0, blocks)
     def _(i):
-        rows = pl.ds(pl.multiple_of(i * small, small), small)
-        total = mid[rows, :].astype(F32) + (part[0, rows, :].astype(F32) + prec[rows, :].astype(F32))
-        out_ref[rows, :] = total.astype(BF16)
-        sq_send[rows, :] = jnp.broadcast_to(jnp.sum(total * total, axis=1, keepdims=True), (small, 128))
-
-    swap_sq = swap(sq_send, sq_recv, 1 + 2 * blocks + half_n)
-    swap_sq.start()
-    swap_sq.wait()
-    scale_ref[...] = lax.rsqrt((sq_send[...] + sq_recv[...]) / (2 * half) + epsilon)
+        total_rows(order[-2], i)
+        total_rows(order[-1], i)
+        swap_sq(i).start()
+
+    @pl.loop(0, blocks)
+    def _(i):
+        swap_sq(i).wait()
+        rows = pl.ds(pl.multiple_of(i * ROWS, ROWS), ROWS)
+        squares = jnp.sum(sq_send[rows, :] + sq_recv[rows, :], axis=1, keepdims=True)
+        scale_ref[rows, :] = jnp.broadcast_to(lax.rsqrt(squares / (2 * half) + epsilon), (ROWS, 128))
 
     @pl.loop(0, n - 1)
     def _(s):
         for k in range(len(views)):
             cw(k, s).wait_send()
             ccw(k, s).wait_send()
-            across(k, s, rep).wait_send()
-
-
-def closing_kernel(total_ref, scale_ref, gain_ref, out_ref):
-    out_ref[...] = (total_ref[...].astype(F32) * scale_ref[:, :1] * gain_ref[...]).astype(BF16)
+            if shared(k):
+                across(k, s, rep).wait_send()
+
+    @pl.loop(0, blocks)
+    def _(i):
+        for j in range(half_n):
+            back_swap(j, i).wait_send()
+            write(j, i).wait()
+
+
+CHUNKS = 8
+
+
+def closing_kernel(total_in, scale_in, gain_ref, out_ref, total, scale, result, sems):
+    rows = total.shape[0] // CHUNKS
+
+    def copies(i):
+        at = pl.ds(i * rows, rows)
+        return (
+            pltpu.make_async_copy(total_in.at[at, :], total.at[at, :], sems.at[0, i]),
+            pltpu.make_async_copy(scale_in.at[at, :], scale.at[at, :], sems.at[1, i]),
+            pltpu.make_async_copy(result.at[at, :], out_ref.at[at, :], sems.at[2, i]),
+        )
+
+    for i in range(CHUNKS):
+        first, second, _ = copies(i)
+        first.start()
+        second.start()
+    for i in range(CHUNKS):
+        first, second, third = copies(i)
+        first.wait()
+        second.wait()
+        at = pl.ds(i * rows, rows)
+        result[at, :] = (total[at, :].astype(F32) * scale[at, :1] * gain_ref[...]).astype(BF16)
+        third.start()
+    for i in range(CHUNKS):
+        copies(i)[2].wait()
 
 
 def fused(n, stream_in, decay_shift, mixer_gain, gate_weight, input_weight, filter_taps, recur_gate,
@@ -495,12 +586,12 @@
     half_n = n // 2
     vmem = pl.BlockSpec(memory_space=pltpu.VMEM)
     hbm = pl.BlockSpec(memory_space=pl.ANY)
-    swaps = 2 + 2 * blocks + half_n
+    swaps = 1 + 2 * blocks + half_n * blocks + blocks
     total, scale = pl.pallas_call(
         functools.partial(layer_kernel, n),
         out_shape=(jax.ShapeDtypeStruct((length, half), BF16), jax.ShapeDtypeStruct((length, 128), F32)),
         in_specs=[hbm, vmem, vmem, hbm, hbm, vmem, vmem, vmem, vmem, hbm, vmem, hbm, hbm],
-        out_specs=(vmem, vmem),
+        out_specs=(hbm, vmem),
         scratch_shapes=[
             pltpu.VMEM((length, half), BF16),
             pltpu.VMEM((model, channels), BF16),
@@ -522,10 +613,11 @@
             pltpu.VMEM((length, 128), F32),
             pltpu.VMEM((length, 128), F32),
             pltpu.SemaphoreType.DMA((6,)),
-            pltpu.SemaphoreType.DMA((7, 3, n - 1)),
-            pltpu.SemaphoreType.DMA((7, 3, n - 1)),
+            pltpu.SemaphoreType.DMA((9, 3, n - 1)),
+            pltpu.SemaphoreType.DMA((9, 3, n - 1)),
             pltpu.SemaphoreType.DMA((swaps,)),
             pltpu.SemaphoreType.DMA((swaps,)),
+            pltpu.SemaphoreType.DMA((half_n * blocks,)),
         ],
         compiler_params=pltpu.CompilerParams(
             collective_id=0, has_side_effects=True, vmem_limit_bytes=67043328
@@ -546,17 +638,17 @@
         up_weight,
         down_weight,
     )
-    tile = pl.BlockSpec((ROWS, half), lambda i: (i, 0))
     out = pl.pallas_call(
         closing_kernel,
-        grid=(blocks,),
         out_shape=jax.ShapeDtypeStruct((length, half), BF16),
-        in_specs=[
-            tile,
-            pl.BlockSpec((ROWS, 128), lambda i: (i, 0)),
-            pl.BlockSpec((1, half), lambda i: (0, 0)),
+        in_specs=[hbm, hbm, vmem],
+        out_specs=hbm,
+        scratch_shapes=[
+            pltpu.VMEM((length, half), BF16),
+            pltpu.VMEM((length, 128), F32),
+            pltpu.VMEM((length, half), BF16),
+            pltpu.SemaphoreType.DMA((3, CHUNKS)),
         ],
-        out_specs=tile,
         name="closing",
     )(total, scale, final_gain.reshape(1, -1))
     return out.reshape(1, length, half)

time: 181 us -> 173 us (0.956)
  Pallas kernels: 181 us -> 173 us
    pallas_call x1, Pallas kernels: 177 us -> 169 us  [fused(): pl.pallas_call(functools.partial(layer_kernel, n), out_shape=(jax.ShapeDt...]
where the time goes in v1:
time: 173 us
  Pallas kernels  173 us (100%)
    pallas_call x1, Pallas kernels, fused(): pl.pallas_call(functools.partial(layer_kernel, n), out_shape=(jax.ShapeDt...  169 us
    pallas_call x1, Pallas kernels, fused(): pl.pallas_call(closing_kernel, out_shape=jax.ShapeDtypeStruct((length, ha...  3.5 us

profile of v1, /device:TPU:0, one launch (start us, length us, event | category | flops | bytes accessed | tf_op | source)
XLA Modules:
  0.0 172.8 jit_solution(4264571772516828966)
XLA Ops:
  0.0 169.3 %gated_layer.1 = (bf16[1024,1024]{1,0:T(8,128)(2,1)}, f32[1024,128]{1,0:T(8,128)}) custom-call(bf16[1024,1024]{1,0:T(8,128)(2,1)} %bitcast.6, f32[1,1024]{1,0:T(1,128)} %shift_ref.1, f32[1,2048]{1,0:T(1,128)} %bitcast.7, bf16[256,512]{1,0:T(8,128)(2,1)} %wg_in.1, bf16[256,512]{1,0:T(8,128)(2,1)} %wi_in.1, f32[4,512]{1,0:T(4,128)} %taps_ref.1, ...), custom_call_target="tpu_custom_call" | custom-call | tf_op jit(solution)/shard_map/gated_layer/pallas_call | solution.py:590
  169.3 3.5 %closing.1 = bf16[1024,1024]{1,0:T(8,128)(2,1)} custom-call(bf16[1024,1024]{1,0:T(8,128)(2,1)} %get-tuple-element.7.total_in, f32[1024,128]{1,0:T(8,128)} %get-tuple-element.8.scale_in, f32[1,1024]{1,0:T(1,128)} %bitcast.9), custom_call_target="tpu_custom_call" | custom-call | tf_op jit(solution)/shard_map/closing/pallas_call | solution.py:641

commit v2 on v1

--- a/solution.py
+++ b/solution.py
@@ -155,11 +155,12 @@
 
 def layer_kernel(
     n,
-    x_in, shift_ref, mgain_ref, wg_in, wi_in, taps_ref, rg_ref, ig_ref, sp_ref, wo_in,
-    fgain_ref, wu_in, wd_in,
+    x_in, shift_in, mgain_in, wg_in, wi_in, taps_in, rg_in, ig_in, sp_in, wo_in,
+    fgain_in, wu_in, wd_in, lgain_in,
     out_ref, scale_ref,
+    shift_ref, mgain_ref, taps_ref, rg_ref, ig_ref, sp_ref, fgain_ref, lgain_ref,
     x_ref, wg, wi, wo, wu, wd, other, normed, front, carry, scan_a, scan_b, part, prec, mid, mid_other,
-    act, sq_send, sq_recv,
+    act, sq_send, sq_recv, acc, scales,
     local_sems, send_sems, recv_sems, tp_send, tp_recv, out_sems,
 ):
     rep, fs, tp = lax.axis_index("rep"), lax.axis_index("fs"), lax.axis_index("tp")
@@ -190,20 +191,24 @@
         return view
 
     rows_o, rows_d = wo.shape[1], wd.shape[1]
-    cut = hidden * 3 // 8
-    rest = (hidden - cut) // 2
-    last = rows_d // 16
-    main = (rows_d - 2 * last) // 2
+    def plain_split(rows, up):
+        p, q = split_rows(rows, up)
+        return (0, p), (p, q)
+
+    quarter = hidden // 4
+    half_d = rows_d // 2
+    private, last = rows_d // 8, rows_d // 16
+    common = half_d - 2 * private - last
     views = [
-        (by_row(wg, 0, channels), BACK, split_rows(shard, True)),
-        (by_row(wi, 0, channels), FORE, split_rows(shard, True)),
-        (by_owner(wo, 0), FORE, split_rows(rows_o, False)),
-        (by_row(wu, 0, cut), BACK, split_rows(shard, True)),
-        (by_row(wu, cut, rest), FORE, split_rows(shard, True)),
-        (by_row(wu, cut + rest, rest), BACK, split_rows(shard, False)),
-        (by_owner(wd, 0), FORE, split_rows(main, False)),
-        (by_owner(wd, main), BACK, split_rows(main, False)),
-        (by_owner(wd, 2 * main), BOTH, (last, last)),
+        (by_row(wg, 0, channels), BACK, plain_split(shard, True)),
+        (by_row(wi, 0, channels), FORE, plain_split(shard, True)),
+        (by_owner(wo, 0), FORE, plain_split(rows_o, True)),
+        (by_row(wu, 0, quarter), BACK, plain_split(shard, True)),
+        (by_row(wu, quarter, 2 * quarter), FORE, plain_split(shard, True)),
+        (by_row(wu, 3 * quarter, quarter), BACK, plain_split(shard, True)),
+        (by_owner(wd, 0), FORE, ((0, common), (half_d, private))),
+        (by_owner(wd, 0), BACK, ((half_d + 2 * private, common), (common + last, private))),
+        (by_owner(wd, 0), BOTH, ((common, last), (rows_d - last, last))),
     ]
     ups = range(3, 6)
     downs = range(6, 9)
@@ -216,19 +221,19 @@
         )
 
     def cw(k, s, shift=0):
-        view, role, (p, q) = views[k]
-        lo, size = (p + rep * q, q) if role == BACK else (0, p)
-        return remote(view(ring_to_fs(pos - s - shift), lo, size), k, 0, s, {"fs": right})
+        view, role, (whole, (lo, size)) = views[k]
+        at = (lo + rep * size, size) if role == BACK else whole
+        return remote(view(ring_to_fs(pos - s - shift), *at), k, 0, s, {"fs": right})
 
     def ccw(k, s, shift=0):
-        view, role, (p, q) = views[k]
-        lo, size = (p + rep * q, q) if role == FORE else (p if role == BOTH else 0, q if role == BOTH else p)
-        return remote(view(ring_to_fs(pos + s + shift), lo, size), k, 1, s, {"fs": left})
+        view, role, (whole, (lo, size)) = views[k]
+        at = whole if role == BACK else (lo + rep * size if role == FORE else lo, size)
+        return remote(view(ring_to_fs(pos + s + shift), *at), k, 1, s, {"fs": left})
 
     def across(k, s, side):
-        view, role, (p, q) = views[k]
+        view, role, (_, (lo, size)) = views[k]
         owner = pos + s + 1 if role == FORE else pos - s - 1
-        return remote(view(ring_to_fs(owner), p + side * q, q), k, 2, s, {"rep": 1 - rep})
+        return remote(view(ring_to_fs(owner), lo + side * size, size), k, 2, s, {"rep": 1 - rep})
 
     def shared(k):
         return views[k][1] != BOTH
@@ -270,13 +275,21 @@
         (wo_in, wo.at[fs]),
         (wu_in, wu.at[pl.ds(pl.multiple_of(fs * shard, TILE), shard), :]),
         (wd_in, wd.at[fs]),
+        (mgain_in, mgain_ref),
+        (shift_in, shift_ref),
+        (taps_in, taps_ref),
+        (rg_in, rg_ref),
+        (ig_in, ig_ref),
+        (sp_in, sp_ref),
+        (fgain_in, fgain_ref),
+        (lgain_in, lgain_ref),
     ]
     local = [pltpu.make_async_copy(a, b, local_sems.at[i]) for i, (a, b) in enumerate(own)]
-    for i in (1, 2, 3, 0, 4, 5):
-        local[i].start()
     barrier = pltpu.get_barrier_semaphore()
     for device in ({"fs": right}, {"fs": left}, {"rep": 1 - rep}, {"tp": 1 - tp}):
         pl.semaphore_signal(barrier, inc=1, device_id=device, device_id_type=pl.DeviceIdType.MESH)
+    for i in (1, 2, 3, 0, 4, 5, *range(6, len(own))):
+        local[i].start()
     pl.semaphore_wait(barrier, 4)
     swap_x = swap(x_ref, other, 0)
     for k in range(3):
@@ -284,8 +297,8 @@
         begin(k)
     local[0].wait()
     swap_x.start()
-    local[4].wait()
-    local[5].wait()
+    for i in range(4, len(own)):
+        local[i].wait()
 
     own_cols = pl.ds(pl.multiple_of(tp * half, 128), half)
     other_cols = pl.ds(pl.multiple_of((1 - tp) * half, 128), half)
@@ -426,7 +439,7 @@
         tick(blocks + 2, part_of)
 
     tick(blocks + 2, 2)
-    for t in range(blocks + 3, n):
+    for t in range(blocks + 3, n + 1):
         for j in range(3):
             tick(t, j)
 
@@ -447,9 +460,9 @@
             act[rows, to] = (up * up).astype(BF16)
 
         for j in range(3):
-            pl.when(c == j)(functools.partial(tick, n, j))
-
-    tick(n + 1, 0)
+            pl.when(c == j)(functools.partial(tick, n + 1, j))
+
+    tick(n + 2, 0)
 
     def place(owner, i):
         column = lax.rem(owner, half_n)
@@ -471,6 +484,18 @@
         part[slot, rows, to] = jnp.dot(act[rows, :], wd[owner], preferred_element_type=F32).astype(BF16)
         pl.when(slot == 1)(lambda: back_swap(column, i).start())
 
+    def early_rows(e, owner, i):
+        rows = pl.ds(pl.multiple_of(i * ROWS, ROWS), ROWS)
+        take = pl.ds((1 - e) * half_d, half_d)
+        acc[e, rows, :] = jnp.dot(act[rows, take], wd[owner, take, :], preferred_element_type=F32)
+
+    def late_rows(e, owner, i):
+        column, slot, rows, to = place(owner, i)
+        take = pl.ds(e * half_d, half_d)
+        rest = jnp.dot(act[rows, take], wd[owner, take, :], preferred_element_type=F32)
+        part[slot, rows, to] = (acc[e, rows, :] + rest).astype(BF16)
+        pl.when(slot == 1)(lambda: back_swap(column, i).start())
+
     def total_rows(owner, i):
         column, slot, rows, to = place(owner, i)
 
@@ -478,7 +503,7 @@
         def _():
             back_swap(column, i).wait_recv()
             total = mid[rows, to].astype(F32) + (part[0, rows, to].astype(F32) + prec[rows, to].astype(F32))
-            other[rows, to] = total.astype(BF16)
+            other[rows, to] = (total * lgain_ref[:, to]).astype(BF16)
             squares = total * total
             sq_send[rows, :] += sum(squares[:, at : at + 128] for at in range(0, width, 128))
             write(column, i).start()
@@ -494,7 +519,7 @@
         order += [ring_to_fs(pos - s - 1), ring_to_fs(pos + s + 1)]
     sq_send[...] = jnp.zeros_like(sq_send)
     over_rows((down_rows, order[0]))
-    for at in range(3 * n + 4, 3 * (lead + half_n + 1)):
+    for at in range(3 * n + 7, 3 * (lead + half_n + 1)):
         tick(at // 3, at % 3)
     for s in range(half_n - 1, n - 1):
         ahead = lead + s + 2
@@ -512,24 +537,38 @@
         if s < n - 3:
             for j in range(1 if s >= half_n else 0, 3):
                 tick(ahead, j)
-    over_rows((down_rows, order[-2]), (down_rows, order[-1]), (total_rows, order[-3]))
+                if s == half_n - 1 and j < 2:
+                    over_rows((functools.partial(early_rows, j), order[j - 2]))
 
     def swap_sq(i):
         rows = pl.ds(pl.multiple_of(i * ROWS, ROWS), ROWS)
         return swap(sq_send.at[rows, :], sq_recv.at[rows, :], 1 + 2 * blocks + half_n * blocks + i)
 
-    @pl.loop(0, blocks)
-    def _(i):
+    def settle(i):
         total_rows(order[-2], i)
         total_rows(order[-1], i)
         swap_sq(i).start()
+
+    @pl.loop(0, blocks)
+    def _(i):
+        late_rows(0, order[-2], i)
+        late_rows(1, order[-1], i)
+        total_rows(order[-3], i)
+        pl.when(i > 0)(lambda: settle(i - 1))
+
+    settle(blocks - 1)
+
+    def write_scale(i):
+        rows = pl.ds(pl.multiple_of(i * ROWS, ROWS), ROWS)
+        return pltpu.make_async_copy(scales.at[rows, :], scale_ref.at[rows, :], out_sems.at[half_n * blocks + i])
 
     @pl.loop(0, blocks)
     def _(i):
         swap_sq(i).wait()
         rows = pl.ds(pl.multiple_of(i * ROWS, ROWS), ROWS)
         squares = jnp.sum(sq_send[rows, :] + sq_recv[rows, :], axis=1, keepdims=True)
-        scale_ref[rows, :] = jnp.broadcast_to(lax.rsqrt(squares / (2 * half) + epsilon), (ROWS, 128))
+        scales[rows, :] = jnp.broadcast_to(lax.rsqrt(squares / (2 * half) + epsilon), (ROWS, 128))
+        write_scale(i).start()
 
     @pl.loop(0, n - 1)
     def _(s):
@@ -544,12 +583,13 @@
         for j in range(half_n):
             back_swap(j, i).wait_send()
             write(j, i).wait()
+        write_scale(i).wait()
 
 
 CHUNKS = 8
 
 
-def closing_kernel(total_in, scale_in, gain_ref, out_ref, total, scale, result, sems):
+def closing_kernel(total_in, scale_in, out_ref, total, scale, result, sems):
     rows = total.shape[0] // CHUNKS
 
     def copies(i):
@@ -569,7 +609,7 @@
         first.wait()
         second.wait()
         at = pl.ds(i * rows, rows)
-        result[at, :] = (total[at, :].astype(F32) * scale[at, :1] * gain_ref[...]).astype(BF16)
+        result[at, :] = (total[at, :].astype(F32) * scale[at, :1]).astype(BF16)
         third.start()
     for i in range(CHUNKS):
         copies(i)[2].wait()
@@ -590,9 +630,17 @@
     total, scale = pl.pallas_call(
         functools.partial(layer_kernel, n),
         out_shape=(jax.ShapeDtypeStruct((length, half), BF16), jax.ShapeDtypeStruct((length, 128), F32)),
-        in_specs=[hbm, vmem, vmem, hbm, hbm, vmem, vmem, vmem, vmem, hbm, vmem, hbm, hbm],
-        out_specs=(hbm, vmem),
+        in_specs=[hbm] * 14,
+        out_specs=(hbm, hbm),
         scratch_shapes=[
+            pltpu.VMEM((1, length), F32),
+            pltpu.VMEM((1, model), F32),
+            pltpu.VMEM(filter_taps.shape, F32),
+            pltpu.VMEM(recur_gate.shape, BF16),
+            pltpu.VMEM(inlet_gate.shape, BF16),
+            pltpu.VMEM((1, channels), F32),
+            pltpu.VMEM((1, model), F32),
+            pltpu.VMEM((1, half), F32),
             pltpu.VMEM((length, half), BF16),
             pltpu.VMEM((model, channels), BF16),
             pltpu.VMEM((model, channels), BF16),
@@ -612,12 +660,14 @@
             pltpu.VMEM((length, hidden), BF16),
             pltpu.VMEM((length, 128), F32),
             pltpu.VMEM((length, 128), F32),
-            pltpu.SemaphoreType.DMA((6,)),
+            pltpu.VMEM((2, length, width), F32),
+            pltpu.VMEM((length, 128), F32),
+            pltpu.SemaphoreType.DMA((14,)),
             pltpu.SemaphoreType.DMA((9, 3, n - 1)),
             pltpu.SemaphoreType.DMA((9, 3, n - 1)),
             pltpu.SemaphoreType.DMA((swaps,)),
             pltpu.SemaphoreType.DMA((swaps,)),
-            pltpu.SemaphoreType.DMA((half_n * blocks,)),
+            pltpu.SemaphoreType.DMA((half_n * blocks + blocks,)),
         ],
         compiler_params=pltpu.CompilerParams(
             collective_id=0, has_side_effects=True, vmem_limit_bytes=67043328
@@ -637,11 +687,12 @@
         feedforward_gain.reshape(1, -1),
         up_weight,
         down_weight,
+        final_gain.reshape(1, -1),
     )
     out = pl.pallas_call(
         closing_kernel,
         out_shape=jax.ShapeDtypeStruct((length, half), BF16),
-        in_specs=[hbm, hbm, vmem],
+        in_specs=[hbm, hbm],
         out_specs=hbm,
         scratch_shapes=[
             pltpu.VMEM((length, half), BF16),
@@ -650,7 +701,7 @@
             pltpu.SemaphoreType.DMA((3, CHUNKS)),
         ],
         name="closing",
-    )(total, scale, final_gain.reshape(1, -1))
+    )(total, scale)
     return out.reshape(1, length, half)
 
 

time: 173 us -> 168 us (0.971)
  Pallas kernels: 173 us -> 168 us
    pallas_call x1, Pallas kernels: 169 us -> 165 us  [fused(): pl.pallas_call(functools.partial(layer_kernel, n), out_shape=(jax.ShapeDt...]
where the time goes in v2:
time: 168 us
  Pallas kernels  168 us (100%)
    pallas_call x1, Pallas kernels, fused(): pl.pallas_call(functools.partial(layer_kernel, n), out_shape=(jax.ShapeDt...  165 us

profile of v2, /device:TPU:0, one launch (start us, length us, event | category | flops | bytes accessed | tf_op | source)
XLA Modules:
  0.0 168.1 jit_solution(4608813020655177368)
XLA Ops:
  0.0 165.4 %gated_layer.1 = (bf16[1024,1024]{1,0:T(8,128)(2,1)}, f32[1024,128]{1,0:T(8,128)}) custom-call(bf16[1024,1024]{1,0:T(8,128)(2,1)} %bitcast.6, f32[1,1024]{1,0:T(1,128)} %shift_in.1, f32[1,2048]{1,0:T(1,128)} %bitcast.7, bf16[256,512]{1,0:T(8,128)(2,1)} %wg_in.1, bf16[256,512]{1,0:T(8,128)(2,1)} %wi_in.1, f32[4,512]{1,0:T(4,128)} %taps_in.1, ...), custom_call_target="tpu_custom_call" | custom-call | tf_op jit(solution)/shard_map/gated_layer/pallas_call | solution.py:630
  165.4 2.7 %closing.1 = bf16[1024,1024]{1,0:T(8,128)(2,1)} custom-call(bf16[1024,1024]{1,0:T(8,128)(2,1)} %get-tuple-element.7.total_in, f32[1024,128]{1,0:T(8,128)} %get-tuple-element.8.scale_in), custom_call_target="tpu_custom_call" | custom-call | tf_op jit(solution)/shard_map/closing/pallas_call | solution.py:692

commit v3 on v2

--- a/solution.py
+++ b/solution.py
@@ -242,21 +242,20 @@
         cw(k, 0).start()
         ccw(k, 0).start()
 
-    def service(k, s, last):
-        def forward(make):
+    def service(turns, s, last):
+        for make, k in turns:
+            make(k, s, 1).wait_recv()
             if last is None:
-                pl.when(s + 1 < n - 1)(lambda: make(k, s + 1).start())
+                pl.when(s + 1 < n - 1)(functools.partial(lambda make, k: make(k, s + 1).start(), make, k))
             elif not last:
                 make(k, s + 1).start()
-
-        cw(k, s, 1).wait_recv()
-        forward(cw)
-        if views[k][1] == BACK:
-            across(k, s, rep).start()
-        ccw(k, s, 1).wait_recv()
-        forward(ccw)
-        if views[k][1] == FORE:
-            across(k, s, rep).start()
+            if views[k][1] == (BACK if make is cw else FORE):
+                across(k, s, rep).start()
+
+    def turns_of(back, fore, third):
+        return [[(cw, back), (ccw, fore)], [(cw, fore), (ccw, back)], [(cw, third), (ccw, third)]]
+
+    mixer_turns, up_turns, down_turns = turns_of(0, 1, 2), turns_of(3, 4, 5), turns_of(7, 6, 8)
 
     def wait_across(k, s):
         if shared(k):
@@ -294,7 +293,9 @@
     swap_x = swap(x_ref, other, 0)
     for k in range(3):
         local[1 + k].wait()
-        begin(k)
+    for turns in mixer_turns:
+        for make, k in turns:
+            make(k, 0).start()
     local[0].wait()
     swap_x.start()
     for i in range(4, len(own)):
@@ -318,11 +319,15 @@
 
     @pl.loop(0, n - 2)
     def _(s):
-        for k in range(3):
-            service(k, s, False)
+        for turns in mixer_turns:
+            service(turns, s, False)
         pl.when(s == 0)(swap_x.wait)
-        for k in list(ups)[:2]:
-            pl.when(s == n - 3)(functools.partial(begin, k))
+
+        @pl.when(s == n - 3)
+        def _():
+            for make, k in up_turns[0] + up_turns[1]:
+                make(k, 0).start()
+
         for piece in range(share):
             i = s * share + piece
 
@@ -331,17 +336,28 @@
                 norm_block(x_ref, other, mgain_ref, pl.ds(pl.multiple_of(i * small, small), small))
 
     begin(ups[-1])
-    for k in range(3):
-        service(k, n - 2, True)
+    for turns in mixer_turns:
+        service(turns, n - 2, True)
 
     lead = n - 2
 
     def tick(t, j):
-        pl.when(t < n - 1)(lambda: service(ups[j], t, None))
+        pl.when(t < n - 1)(lambda: service(up_turns[j], t, None))
+
         if j == 2:
-            for e, k in enumerate(downs):
-                pl.when(t == (n - 4 if e == 0 else n - 3))(functools.partial(begin, k))
-        pl.when(t >= lead)(lambda: service(downs[j], t - lead, None))
+
+            @pl.when(t == n - 4)
+            def _():
+                for make, k in down_turns[0]:
+                    make(k, 0).start()
+
+            @pl.when(t == n - 3)
+            def _():
+                for make, k in down_turns[1]:
+                    make(k, 0).start()
+                begin(downs[2])
+
+        pl.when(t >= lead)(lambda: service(down_turns[j], t - lead, None))
 
     for j in range(3):
         tick(0, j)
@@ -521,24 +537,23 @@
     over_rows((down_rows, order[0]))
     for at in range(3 * n + 7, 3 * (lead + half_n + 1)):
         tick(at // 3, at % 3)
-    for s in range(half_n - 1, n - 1):
-        ahead = lead + s + 2
-        for earlier in range(half_n) if s == half_n - 1 else [s]:
-            for k in downs:
-                wait_across(k, earlier)
-        if s == half_n - 1:
-            over_rows((down_rows, order[1]), (total_rows, order[0]))
-        elif s < n - 2:
-            at = 2 * (s - half_n + 1)
-            over_rows((down_rows, order[at]), (total_rows, order[at - 1]))
-            if s < n - 3:
-                tick(ahead, 0)
-            over_rows((down_rows, order[at + 1]), (total_rows, order[at]))
-        if s < n - 3:
-            for j in range(1 if s >= half_n else 0, 3):
-                tick(ahead, j)
-                if s == half_n - 1 and j < 2:
-                    over_rows((functools.partial(early_rows, j), order[j - 2]))
+    for s in range(half_n):
+        for k in downs:
+            wait_across(k, s)
+    over_rows((down_rows, order[1]), (total_rows, order[0]))
+    for e in range(2):
+        over_rows((functools.partial(early_rows, e), order[e - 2]))
+    for s in range(half_n, n - 2):
+        at = 2 * (s - half_n + 1)
+        tick(lead + s + 1, 0)
+        for k in downs:
+            wait_across(k, s)
+        over_rows((down_rows, order[at]), (total_rows, order[at - 1]))
+        tick(lead + s + 1, 1)
+        over_rows((down_rows, order[at + 1]), (total_rows, order[at]))
+        tick(lead + s + 1, 2)
+    for k in downs:
+        wait_across(k, n - 2)
 
     def swap_sq(i):
         rows = pl.ds(pl.multiple_of(i * ROWS, ROWS), ROWS)

time: 168 us -> 166 us (0.988)
  Pallas kernels: 168 us -> 166 us
    pallas_call x1, Pallas kernels: 165 us -> 163 us  [fused(): pl.pallas_call(functools.partial(layer_kernel, n), out_shape=(jax.ShapeDt...]
where the time goes in v3:
time: 166 us
  Pallas kernels  166 us (100%)
    pallas_call x1, Pallas kernels, fused(): pl.pallas_call(functools.partial(layer_kernel, n), out_shape=(jax.ShapeDt...  163 us

profile of v3, /device:TPU:0, one launch (start us, length us, event | category | flops | bytes accessed | tf_op | source)
XLA Modules:
  0.0 165.6 jit_solution(6890238366198176537)
XLA Ops:
  0.0 162.9 %gated_layer.1 = (bf16[1024,1024]{1,0:T(8,128)(2,1)}, f32[1024,128]{1,0:T(8,128)}) custom-call(bf16[1024,1024]{1,0:T(8,128)(2,1)} %bitcast.6, f32[1,1024]{1,0:T(1,128)} %shift_in.1, f32[1,2048]{1,0:T(1,128)} %bitcast.7, bf16[256,512]{1,0:T(8,128)(2,1)} %wg_in.1, bf16[256,512]{1,0:T(8,128)(2,1)} %wi_in.1, f32[4,512]{1,0:T(4,128)} %taps_in.1, ...), custom_call_target="tpu_custom_call" | custom-call | tf_op jit(solution)/shard_map/gated_layer/pallas_call | solution.py:645
  162.9 2.7 %closing.1 = bf16[1024,1024]{1,0:T(8,128)(2,1)} custom-call(bf16[1024,1024]{1,0:T(8,128)(2,1)} %get-tuple-element.7.total_in, f32[1024,128]{1,0:T(8,128)} %get-tuple-element.8.scale_in), custom_call_target="tpu_custom_call" | custom-call | tf_op jit(solution)/shard_map/closing/pallas_call | solution.py:707

commit v4 on v3

--- a/solution.py
+++ b/solution.py
@@ -215,7 +215,7 @@
 
     def remote(view, k, lane, s, device):
         return pltpu.make_async_remote_copy(
-            src_ref=view, dst_ref=view, send_sem=send_sems.at[k, lane, s],
+            src_ref=view, dst_ref=view, send_sem=send_sems.at[k, lane, lax.rem(s, 2)],
             recv_sem=recv_sems.at[k, lane, s], device_id=device,
             device_id_type=pl.DeviceIdType.MESH,
         )
@@ -242,15 +242,19 @@
         cw(k, 0).start()
         ccw(k, 0).start()
 
+    def launch(make, k, s, *side):
+        pl.when(s >= 2)(lambda: make(k, s - 2, *side).wait_send())
+        make(k, s, *side).start()
+
     def service(turns, s, last):
         for make, k in turns:
             make(k, s, 1).wait_recv()
             if last is None:
-                pl.when(s + 1 < n - 1)(functools.partial(lambda make, k: make(k, s + 1).start(), make, k))
+                pl.when(s + 1 < n - 1)(functools.partial(launch, make, k, s + 1))
             elif not last:
-                make(k, s + 1).start()
+                launch(make, k, s + 1)
             if views[k][1] == (BACK if make is cw else FORE):
-                across(k, s, rep).start()
+                launch(across, k, s, rep)
 
     def turns_of(back, fore, third):
         return [[(cw, back), (ccw, fore)], [(cw, fore), (ccw, back)], [(cw, third), (ccw, third)]]
@@ -552,8 +556,9 @@
         tick(lead + s + 1, 1)
         over_rows((down_rows, order[at + 1]), (total_rows, order[at]))
         tick(lead + s + 1, 2)
-    for k in downs:
-        wait_across(k, n - 2)
+    wait_across(downs[1], n - 2)
+    over_rows((functools.partial(late_rows, 0), order[-2]), (total_rows, order[-3]))
+    wait_across(downs[0], n - 2)
 
     def swap_sq(i):
         rows = pl.ds(pl.multiple_of(i * ROWS, ROWS), ROWS)
@@ -566,9 +571,7 @@
 
     @pl.loop(0, blocks)
     def _(i):
-        late_rows(0, order[-2], i)
         late_rows(1, order[-1], i)
-        total_rows(order[-3], i)
         pl.when(i > 0)(lambda: settle(i - 1))
 
     settle(blocks - 1)
@@ -585,7 +588,7 @@
         scales[rows, :] = jnp.broadcast_to(lax.rsqrt(squares / (2 * half) + epsilon), (ROWS, 128))
         write_scale(i).start()
 
-    @pl.loop(0, n - 1)
+    @pl.loop(n - 3, n - 1)
     def _(s):
         for k in range(len(views)):
             cw(k, s).wait_send()
@@ -678,7 +681,7 @@
             pltpu.VMEM((2, length, width), F32),
             pltpu.VMEM((length, 128), F32),
             pltpu.SemaphoreType.DMA((14,)),
-            pltpu.SemaphoreType.DMA((9, 3, n - 1)),
+            pltpu.SemaphoreType.DMA((9, 3, 2)),
             pltpu.SemaphoreType.DMA((9, 3, n - 1)),
             pltpu.SemaphoreType.DMA((swaps,)),
             pltpu.SemaphoreType.DMA((swaps,)),

time: 166 us -> 164 us (0.988)
  Pallas kernels: 166 us -> 163 us
    pallas_call x1, Pallas kernels: 163 us -> 161 us  [fused(): pl.pallas_call(functools.partial(layer_kernel, n), out_shape=(jax.ShapeDt...]
where the time goes in v4:
time: 164 us; the launch traced here: 163 us
  Pallas kernels  163 us (99%)
    pallas_call x1, Pallas kernels, fused(): pl.pallas_call(functools.partial(layer_kernel, n), out_shape=(jax.ShapeDt...  161 us

profile of v4, /device:TPU:0, one launch (start us, length us, event | category | flops | bytes accessed | tf_op | source)
XLA Modules:
  0.0 163.4 jit_solution(3904935162667333138)
XLA Ops:
  0.0 160.8 %gated_layer.1 = (bf16[1024,1024]{1,0:T(8,128)(2,1)}, f32[1024,128]{1,0:T(8,128)}) custom-call(bf16[1024,1024]{1,0:T(8,128)(2,1)} %bitcast.6, f32[1,1024]{1,0:T(1,128)} %shift_in.1, f32[1,2048]{1,0:T(1,128)} %bitcast.7, bf16[256,512]{1,0:T(8,128)(2,1)} %wg_in.1, bf16[256,512]{1,0:T(8,128)(2,1)} %wi_in.1, f32[4,512]{1,0:T(4,128)} %taps_in.1, ...), custom_call_target="tpu_custom_call" | custom-call | tf_op jit(solution)/shard_map/gated_layer/pallas_call | solution.py:648
  160.8 2.7 %closing.1 = bf16[1024,1024]{1,0:T(8,128)(2,1)} custom-call(bf16[1024,1024]{1,0:T(8,128)(2,1)} %get-tuple-element.7.total_in, f32[1024,128]{1,0:T(8,128)} %get-tuple-element.8.scale_in), custom_call_target="tpu_custom_call" | custom-call | tf_op jit(solution)/shard_map/closing/pallas_call | solution.py:710

commit v5 on v4

--- a/solution.py
+++ b/solution.py
@@ -161,7 +161,7 @@
     shift_ref, mgain_ref, taps_ref, rg_ref, ig_ref, sp_ref, fgain_ref, lgain_ref,
     x_ref, wg, wi, wo, wu, wd, other, normed, front, carry, scan_a, scan_b, part, prec, mid, mid_other,
     act, sq_send, sq_recv, acc, scales,
-    local_sems, send_sems, recv_sems, tp_send, tp_recv, out_sems,
+    local_sems, send_sems, recv_sems, across_sems, tp_send, tp_recv, out_sems,
 ):
     rep, fs, tp = lax.axis_index("rep"), lax.axis_index("fs"), lax.axis_index("tp")
     half_n = n // 2
@@ -216,7 +216,7 @@
     def remote(view, k, lane, s, device):
         return pltpu.make_async_remote_copy(
             src_ref=view, dst_ref=view, send_sem=send_sems.at[k, lane, lax.rem(s, 2)],
-            recv_sem=recv_sems.at[k, lane, s], device_id=device,
+            recv_sem=across_sems.at[k, s] if lane == 2 else recv_sems.at[k, lane, lax.rem(s, 4)], device_id=device,
             device_id_type=pl.DeviceIdType.MESH,
         )
 
@@ -327,7 +327,7 @@
             service(turns, s, False)
         pl.when(s == 0)(swap_x.wait)
 
-        @pl.when(s == n - 3)
+        @pl.when(s == n - 4)
         def _():
             for make, k in up_turns[0] + up_turns[1]:
                 make(k, 0).start()
@@ -350,12 +350,12 @@
 
         if j == 2:
 
-            @pl.when(t == n - 4)
+            @pl.when(t == n - 5)
             def _():
                 for make, k in down_turns[0]:
                     make(k, 0).start()
 
-            @pl.when(t == n - 3)
+            @pl.when(t == n - 4)
             def _():
                 for make, k in down_turns[1]:
                     make(k, 0).start()
@@ -497,7 +497,7 @@
 
     def write(column, i):
         _, _, rows, to = place(column, i)
-        return pltpu.make_async_copy(other.at[rows, to], out_ref.at[rows, to], out_sems.at[column * blocks + i])
+        return pltpu.make_async_copy(other.at[rows, to], out_ref.at[rows, to], out_sems.at[column])
 
     def down_rows(owner, i):
         column, slot, rows, to = place(owner, i)
@@ -578,7 +578,7 @@
 
     def write_scale(i):
         rows = pl.ds(pl.multiple_of(i * ROWS, ROWS), ROWS)
-        return pltpu.make_async_copy(scales.at[rows, :], scale_ref.at[rows, :], out_sems.at[half_n * blocks + i])
+        return pltpu.make_async_copy(scales.at[rows, :], scale_ref.at[rows, :], out_sems.at[half_n])
 
     @pl.loop(0, blocks)
     def _(i):
@@ -596,12 +596,15 @@
             if shared(k):
                 across(k, s, rep).wait_send()
 
+    for j in range(half_n):
+        to = pl.ds(j * width, width)
+        pltpu.make_async_copy(other.at[:, to], out_ref.at[:, to], out_sems.at[j]).wait()
+    pltpu.make_async_copy(scales, scale_ref, out_sems.at[half_n]).wait()
+
     @pl.loop(0, blocks)
     def _(i):
         for j in range(half_n):
             back_swap(j, i).wait_send()
-            write(j, i).wait()
-        write_scale(i).wait()
 
 
 CHUNKS = 8
@@ -682,10 +685,11 @@
             pltpu.VMEM((length, 128), F32),
             pltpu.SemaphoreType.DMA((14,)),
             pltpu.SemaphoreType.DMA((9, 3, 2)),
-            pltpu.SemaphoreType.DMA((9, 3, n - 1)),
+            pltpu.SemaphoreType.DMA((9, 2, 4)),
+            pltpu.SemaphoreType.DMA((8, n - 1)),
             pltpu.SemaphoreType.DMA((swaps,)),
             pltpu.SemaphoreType.DMA((swaps,)),
-            pltpu.SemaphoreType.DMA((half_n * blocks + blocks,)),
+            pltpu.SemaphoreType.DMA((half_n + 1,)),
         ],
         compiler_params=pltpu.CompilerParams(
             collective_id=0, has_side_effects=True, vmem_limit_bytes=67043328

time: 164 us -> 163 us (level)
  no operation moved by 1% of the time
where the time goes in v5:
time: 163 us
  Pallas kernels  163 us (100%)
    pallas_call x1, Pallas kernels, fused(): pl.pallas_call(functools.partial(layer_kernel, n), out_shape=(jax.ShapeDt...  160 us

profile of v5, /device:TPU:0, one launch (start us, length us, event | category | flops | bytes accessed | tf_op | source)
XLA Modules:
  0.0 162.8 jit_solution(13986001672562739524)
XLA Ops:
  0.0 160.1 %gated_layer.1 = (bf16[1024,1024]{1,0:T(8,128)(2,1)}, f32[1024,128]{1,0:T(8,128)}) custom-call(bf16[1024,1024]{1,0:T(8,128)(2,1)} %bitcast.6, f32[1,1024]{1,0:T(1,128)} %shift_in.1, f32[1,2048]{1,0:T(1,128)} %bitcast.7, bf16[256,512]{1,0:T(8,128)(2,1)} %wg_in.1, bf16[256,512]{1,0:T(8,128)(2,1)} %wi_in.1, f32[4,512]{1,0:T(4,128)} %taps_in.1, ...), custom_call_target="tpu_custom_call" | custom-call | tf_op jit(solution)/shard_map/gated_layer/pallas_call | solution.py:651
  160.1 2.7 %closing.1 = bf16[1024,1024]{1,0:T(8,128)(2,1)} custom-call(bf16[1024,1024]{1,0:T(8,128)(2,1)} %get-tuple-element.7.total_in, f32[1024,128]{1,0:T(8,128)} %get-tuple-element.8.scale_in), custom_call_target="tpu_custom_call" | custom-call | tf_op jit(solution)/shard_map/closing/pallas_call | solution.py:714
